TPU v7x, 32 devices: a whole 2x2x4 slice. The times are simulated.
32 devices in a mesh: grp: 2 (over y), sp: 4 (over z), tp: 4 (over x, core).
Axes of the slice: x: 2, y: 2, z: 4, core: 2. Of those that a mesh axis runs over, the one named last changes fastest.
Arguments:
- tokens: bfloat16 [2048, 4096], P(('grp', 'sp')), parts along dimension 0, may hold values from -6 to 6
- norm_gain: bfloat16 [2, 4096], replicated, may hold values from 0.099609375 to 1.8984375
- w_query: bfloat16 [2, 4096, 2048], P(None, 'sp', 'tp'), may hold values from -0.09375 to 0.09375
- w_key: bfloat16 [2, 4096, 2048], P(None, 'sp', 'tp'), may hold values from -0.09375 to 0.09375
- w_value: bfloat16 [2, 4096, 2048], P(None, 'sp', 'tp'), may hold values from -0.09375 to 0.09375
- w_out: bfloat16 [2, 2048, 4096], P(None, 'tp', 'sp'), may hold values from -0.125 to 0.125
- offset_bias: float32 [2, 16, 15, 31], P(None, 'tp'), may hold values from -4 to 300
Outputs:
- mixed: bfloat16 [2048, 4096], P(('grp', 'sp')), parts along dimension 0
There are 2 independent parts, one for each index of `grp`. A program takes and returns all parts, laid end to end along the dimension named above; an argument that names none is the same for every part. Nothing has to cross between parts.
All inputs are finite; a program needn't handle non-finite values.
Results may differ from a plain program's by a relative error of at most 0.013.
Values may be sent and summed in bfloat16 or wider, within the bound.
No kernel may reach another device: no remote copies, remote signals or barrier semaphores. Data moves between devices by JAX's collectives and lax.ppermute only.
A program may use at most 128 MiB of HBM per device.

v0:
```python
import jax
import jax.numpy as jnp
from jax import lax
from jax.sharding import PartitionSpec as P

HD = 128
GRID_W = 64
KR = 8
KC = 16
LAYERS = 2
norm_eps = 1e-06


def with_halo(block, sides, width):
    for axis, dim in sides:
        count = lax.axis_size(axis)
        forward = [(i, i + 1) for i in range(count - 1)]
        backward = [(target, source) for source, target in forward]
        low = lax.ppermute(
            lax.slice_in_dim(block, block.shape[dim] - width, None, axis=dim), axis, forward
        )
        high = lax.ppermute(lax.slice_in_dim(block, 0, width, axis=dim), axis, backward)
        block = jnp.concatenate([low, block, high], axis=dim)
    return block


def rms_rows(values, gain):
    wide = values.astype(jnp.float32)
    scaled = wide * lax.rsqrt(jnp.mean(wide * wide, axis=-1, keepdims=True) + norm_eps)
    return (scaled * gain.astype(jnp.float32)).astype(jnp.bfloat16)


def on_device(tokens, norm_gain, w_query, w_key, w_value, w_out, offset_bias):
    sp_count = lax.axis_size("sp")
    sp_index = lax.axis_index("sp")
    tok_rows = tokens.shape[0]
    local_rows = tok_rows // GRID_W
    grid_rows = local_rows * sp_count
    heads_here = offset_bias.shape[1]
    head_width = heads_here * HD
    reach = KR // 2
    scale = HD ** (-0.5)
    columns = jnp.arange(GRID_W, dtype=jnp.int32)
    col_first = jnp.clip(columns - KC // 2, 0, GRID_W - KC)
    col_inside = (columns[None, :] >= col_first[:, None]) & (
        columns[None, :] < col_first[:, None] + KC
    )
    col_offset = jnp.clip(columns[None, :] - columns[:, None], 1 - KC, KC - 1) + KC - 1
    col_onehot = (
        jnp.arange(2 * KC - 1, dtype=jnp.int32)[:, None, None] == col_offset[None, :, :]
    ).astype(jnp.float32)
    first_row = sp_index * local_rows
    own_rows = first_row + jnp.arange(local_rows, dtype=jnp.int32)
    row_first = jnp.clip(own_rows - reach, 0, grid_rows - KR)
    band_start = row_first - first_row + reach
    row_offset = (
        row_first[:, None] + jnp.arange(KR, dtype=jnp.int32)[None, :] - own_rows[:, None] + KR - 1
    )
    row_onehot = (
        row_offset[:, :, None] == jnp.arange(2 * KR - 1, dtype=jnp.int32)[None, None, :]
    ).astype(jnp.float32)
    every_query, every_key, every_value, every_out = (
        lax.all_gather(w_query, "sp", axis=1, tiled=True),
        lax.all_gather(w_key, "sp", axis=1, tiled=True),
        lax.all_gather(w_value, "sp", axis=1, tiled=True),
        lax.all_gather(w_out, "sp", axis=2, tiled=True),
    )
    residual = tokens
    for layer_index in range(LAYERS):
        normed = rms_rows(residual, norm_gain[layer_index])
        queries = jnp.dot(normed, every_query[layer_index], preferred_element_type=jnp.float32)
        keys = jnp.dot(normed, every_key[layer_index], preferred_element_type=jnp.float32)
        values = jnp.dot(normed, every_value[layer_index], preferred_element_type=jnp.float32)
        out_weight = every_out[layer_index]
        queries = queries.astype(jnp.bfloat16).reshape(local_rows, GRID_W, heads_here, HD)
        key_values = jnp.concatenate(
            [keys.astype(jnp.bfloat16), values.astype(jnp.bfloat16)], axis=1
        )
        key_values = key_values.reshape(local_rows, GRID_W, 2 * head_width)
        padded = with_halo(key_values, (("sp", 0),), reach)
        bands = jax.vmap(lambda band_begin: lax.dynamic_slice_in_dim(padded, band_begin, KR, 0))(
            band_start
        )
        band_keys = bands[..., :head_width].reshape(local_rows, KR, GRID_W, heads_here, HD)
        band_values = bands[..., head_width:].reshape(local_rows, KR, GRID_W, heads_here, HD)
        col_bias = jnp.einsum(
            "hro,oqk->hrqk", offset_bias[layer_index], col_onehot, precision=lax.Precision.HIGHEST
        )
        full_bias = jnp.einsum(
            "ijr,hrqk->hiqjk", row_onehot, col_bias, precision=lax.Precision.HIGHEST
        )
        scores = jnp.einsum(
            "iqhd,ijkhd->hiqjk", queries, band_keys, preferred_element_type=jnp.float32
        )
        scores = scores * scale + full_bias
        scores = jnp.where(col_inside[None, None, :, None, :], scores, -jnp.inf)
        flattened = scores.reshape(heads_here, local_rows, GRID_W, KR * GRID_W)
        weights = jax.nn.softmax(flattened, axis=-1).astype(jnp.bfloat16)
        weights = weights.reshape(heads_here, local_rows, GRID_W, KR, GRID_W)
        attended = jnp.einsum(
            "hiqjk,ijkhd->iqhd", weights, band_values, preferred_element_type=jnp.float32
        )
        attended = attended.astype(jnp.bfloat16).reshape(tok_rows, head_width)
        branch = lax.psum(
            jnp.dot(attended, out_weight, preferred_element_type=jnp.float32).astype(jnp.bfloat16),
            "tp",
        ).astype(jnp.float32)
        residual = (residual.astype(jnp.float32) + branch).astype(jnp.bfloat16)
    return residual


def solution(mesh):
    return jax.shard_map(
        on_device,
        mesh=mesh,
        in_specs=(
            P(("grp", "sp"), None),
            P(),
            P(None, "sp", "tp"),
            P(None, "sp", "tp"),
            P(None, "sp", "tp"),
            P(None, "tp", "sp"),
            P(None, "tp", None, None),
        ),
        out_specs=P(("grp", "sp"), None),
        check_vma=False,
    )
```

profile of v0, /device:TPU:0, one launch (start us, length us, event | category | flops | bytes accessed | tf_op | source)
XLA Modules:
  0.0 783.5 jit_solution(1764364375646308337)
XLA Ops:
  6.5 0.7 all-gather.5.cloned.1.call-update
  7.3 0.7 all-gather.7.cloned.1.call-update
  8.1 0.7 all-gather.9.cloned.1.call-update
  8.8 0.5 all-gather.11.cloned.1.call-update
  9.6 1.0 fusion.73
  10.7 3.8 fusion.30
  14.5 6.0 copy.16
  20.5 0.5 fusion
  21.1 140.2 %all-gather.5.cloned.1.call-done = bf16[2,4096,512]{2,1,0:T(8,128)(2,1)} async-done(((bf16[2,1024,512]{2,1,0:T(8,128)(2,1)}), bf16[2,4096,512]{2,1,0:T(8,128)(2,1)}) %all-gather.5.cloned.1.call-update) | async-done | bytes 8388624 | tf_op jit(solution)/shard_map/all_gather | solution.py:64
  161.3 3.5 fusion.54
  164.7 145.9 %all-gather.7.cloned.1.call-done = bf16[2,4096,512]{2,1,0:T(8,128)(2,1)} async-done(((bf16[2,1024,512]{2,1,0:T(8,128)(2,1)}), bf16[2,4096,512]{2,1,0:T(8,128)(2,1)}) %all-gather.7.cloned.1.call-update) | async-done | bytes 8388624 | tf_op jit(solution)/shard_map/all_gather | solution.py:65
  310.7 3.5 fusion.55
  314.2 2.1 collective-permute-start
  316.3 1.5 collective-permute-start.1
  317.8 149.6 %all-gather.9.cloned.1.call-done = bf16[2,4096,512]{2,1,0:T(8,128)(2,1)} async-done(((bf16[2,1024,512]{2,1,0:T(8,128)(2,1)}), bf16[2,4096,512]{2,1,0:T(8,128)(2,1)}) %all-gather.9.cloned.1.call-update) | async-done | bytes 8388624 | tf_op jit(solution)/shard_map/all_gather | solution.py:63
  467.4 3.5 fusion.56
  471.0 2.5 pad_maximum_fusion
  473.5 4.4 gather_fusion
  477.9 3.5 slice_bitcast_fusion.19
  481.4 0.6 copy-done.2
  482.0 1.0 fusion.93
  483.0 0.7 fusion.16
  483.7 1.0 fusion.60
  484.9 132.0 %all-gather.11.cloned.1.call-done = bf16[2,512,4096]{2,1,0:T(8,128)(2,1)} async-done(((bf16[2,512,1024]{2,1,0:T(8,128)(2,1)}), bf16[2,512,4096]{2,1,0:T(8,128)(2,1)}) %all-gather.11.cloned.1.call-update) | async-done | bytes 8388624 | tf_op jit(solution)/shard_map/all_gather | solution.py:66
  616.9 4.8 convolution_convert_fusion.1
  621.8 2.4 fusion.71
  624.2 47.2 %all-reduce.4.cloned.1.call-done = bf16[256,4096]{1,0:T(8,128)(2,1)} async-done(((bf16[256,4096]{1,0:T(8,128)(2,1)}), bf16[256,4096]{1,0:T(8,128)(2,1)}) %all-reduce.4.cloned.1.call-update) | async-done | bytes 2097168 | tf_op jit(solution)/shard_map/psum | solution.py:104
  671.5 2.5 fusion.4
  674.0 1.0 fusion.6
  675.0 4.5 fusion.57
  679.5 1.2 fusion.58
  680.8 3.4 collective-permute-start.2
  684.3 1.5 collective-permute-start.3
  685.8 3.9 fusion.28
  689.7 5.8 copy.22
  695.4 4.8 fusion.59
  700.2 1.0 reshape.189
  701.3 2.4 pad_maximum_fusion.1
  703.6 4.2 gather_fusion.1
  707.8 3.1 slice_bitcast_fusion.17
  710.9 0.3 copy-done.3
  711.3 1.0 fusion.94
  712.3 0.7 fusion.17
  713.0 1.0 fusion.65
  714.5 1.5 slice-done.1
  715.9 2.6 convolution_convert_fusion
  718.6 53.4 %all-reduce.6.cloned.1.call-done = bf16[256,4096]{1,0:T(8,128)(2,1)} async-done(((bf16[256,4096]{1,0:T(8,128)(2,1)}), bf16[256,4096]{1,0:T(8,128)(2,1)}) %all-reduce.6.cloned.1.call-update) | async-done | bytes 2097168 | tf_op jit(solution)/shard_map/psum | solution.py:104
  771.9 4.7 fusion.7
  (51 shorter events, 1.5 us)
Async XLA Ops:
  6.5 2.9 copy-start.7
  6.5 154.7 %all-gather.5.cloned.1.call-start = ((), (), s32[]{:S(2)}) async-start(), calls=%async_computation | async-start | bytes 10485760 | tf_op jit(solution)/shard_map/all_gather | solution.py:64
  7.3 303.4 %all-gather.7.cloned.1.call-start = ((), (), s32[]{:S(2)}) async-start(), calls=%async_computation.1 | async-start | bytes 10485760 | tf_op jit(solution)/shard_map/all_gather | solution.py:65
  8.0 459.4 %all-gather.9.cloned.1.call-start = ((), (), s32[]{:S(2)}) async-start(), calls=%async_computation.2 | async-start | bytes 10485760 | tf_op jit(solution)/shard_map/all_gather | solution.py:63
  8.7 608.2 %all-gather.11.cloned.1.call-start = ((), (), s32[]{:S(2)}) async-start(), calls=%async_computation.3 | async-start | bytes 10485760 | tf_op jit(solution)/shard_map/all_gather | solution.py:66
  9.3 662.1 %all-reduce.4.cloned.1.call-start = ((), (), s32[]{:S(2)}) async-start(), calls=%async_computation.4 | async-start | bytes 4194304 | tf_op jit(solution)/shard_map/psum | solution.py:104
  14.5 6.0 copy-start
  14.5 6.6 copy-start.6
  314.2 156.7 %collective-permute-start = (bf16[4,64,1024]{2,1,0:T(8,128)(2,1)S(1)}, bf16[4,64,1024]{2,1,0:T(8,128)(2,1)}, u32[]{:S(2)}, u32[]{:S(2)}) collective-permute-start(bf16[4,64,1024]{2,1,0:T(8,128)(2,1)S(1)} %bitcast.150), channel_id=1, source_target_pairs={{0,4},{4,8},{8,12},{1,5},{5,9},{9,13},{2,6},{6,10},{10,14},{3,7},{... | collective-permute-start | bytes 1572872 | tf_op jit(solution)/shard_map/ppermute | solution.py:19
  316.3 154.6 %collective-permute-start.1 = (bf16[4,64,1024]{2,1,0:T(8,128)(2,1)S(1)}, bf16[4,64,1024]{2,1,0:T(8,128)(2,1)}, u32[]{:S(2)}, u32[]{:S(2)}) collective-permute-start(bf16[4,64,1024]{2,1,0:T(8,128)(2,1)S(1)} %bitcast.151), channel_id=1, source_target_pairs={{4,0},{8,4},{12,8},{5,1},{9,5},{13,9},{6,2},{10,6},{14,10},{7,3},{... | collective-permute-start | bytes 1572872 | tf_op jit(solution)/shard_map/ppermute | solution.py:22
  477.9 4.1 copy-start.2
  621.7 150.2 %all-reduce.6.cloned.1.call-start = ((), (), s32[]{:S(2)}) async-start(), calls=%async_computation.5 | async-start | bytes 4194304 | tf_op jit(solution)/shard_map/psum | solution.py:104
  671.5 2.5 copy-start.1
  674.0 5.5 slice-start.2
  674.9 4.5 copy-start.5
  675.0 4.6 slice-start.3
  679.5 6.3 copy-start.4
  680.8 20.4 %collective-permute-start.2 = (bf16[4,64,1024]{2,1,0:T(8,128)(2,1)S(1)}, bf16[4,64,1024]{2,1,0:T(8,128)(2,1)S(1)}, u32[]{:S(2)}, u32[]{:S(2)}) collective-permute-start(bf16[4,64,1024]{2,1,0:T(8,128)(2,1)S(1)} %bitcast.147), channel_id=1, source_target_pairs={{0,4},{4,8},{8,12},{1,5},{5,9},{9,13},{2,6},{6,10},{10,14},{3,7},{... | collective-permute-start | bytes 1572872 | tf_op jit(solution)/shard_map/ppermute | solution.py:19
  684.3 17.0 %collective-permute-start.3 = (bf16[4,64,1024]{2,1,0:T(8,128)(2,1)S(1)}, bf16[4,64,1024]{2,1,0:T(8,128)(2,1)}, u32[]{:S(2)}, u32[]{:S(2)}) collective-permute-start(bf16[4,64,1024]{2,1,0:T(8,128)(2,1)S(1)} %bitcast.148), channel_id=1, source_target_pairs={{4,0},{8,4},{12,8},{5,1},{9,5},{13,9},{6,2},{10,6},{14,10},{7,3},{... | collective-permute-start | bytes 1572872 | tf_op jit(solution)/shard_map/ppermute | solution.py:22
  707.8 3.4 copy-start.3
  712.3 2.2 slice-start
  713.0 2.9 slice-start.1
Sparse Core Ops, SparseCore 0:
  8.9 152.3 all-gather.4
  162.8 147.7 all-gather.6
  312.2 155.1 all-gather.8
  468.8 148.0 all-gather.10
  621.9 49.5 all-reduce.3
  718.7 53.1 all-reduce.5
where the time goes:
time: 784 us; the launch traced here: 783 us
  waiting for transfers between devices  671 us (86%)
  matrix products  43.4 us (6%)
  local copies, waits for them, and re-layouts  31.2 us (4%)
  other arithmetic  15.4 us (2%)
  between operations  13.8 us (2%)
  starting transfers between devices  8.71 us (1%)
    all_gather x1, waiting for transfers between devices, on_device(): lax.all_gather(w_query, 'sp', axis=1, tiled=True)  150 us
    all_gather x1, waiting for transfers between devices, on_device(): lax.all_gather(w_value, 'sp', axis=1, tiled=True)  146 us
    all_gather x1, waiting for transfers between devices, on_device(): lax.all_gather(w_key, 'sp', axis=1, tiled=True)  140 us
    all_gather x1, waiting for transfers between devices, on_device(): lax.all_gather(w_out, 'sp', axis=2, tiled=True)  132 us
    psum x2, waiting for transfers between devices, on_device(): lax.psum(jnp.dot(attended, out_weight, preferred_element_type=jnp.float32...  101 us
  transfers between devices with their start and end apart: 10, of which 6 were waited for; matrix products, arithmetic and copies ran while one was open for 7% of the time, Pallas kernels for 0%

commit v1 on v0

--- a/solution.py
+++ b/solution.py
@@ -101,9 +101,14 @@
             "hiqjk,ijkhd->iqhd", weights, band_values, preferred_element_type=jnp.float32
         )
         attended = attended.astype(jnp.bfloat16).reshape(tok_rows, head_width)
-        branch = lax.psum(
-            jnp.dot(attended, out_weight, preferred_element_type=jnp.float32).astype(jnp.bfloat16),
-            "tp",
+        branch = jnp.sum(
+            lax.all_gather(
+                jnp.dot(attended, out_weight, preferred_element_type=jnp.float32).astype(
+                    jnp.bfloat16
+                ),
+                "tp",
+            ),
+            axis=0,
         ).astype(jnp.float32)
         residual = (residual.astype(jnp.float32) + branch).astype(jnp.bfloat16)
     return residual

time: 784 us -> 812 us (1.036)
  other arithmetic: 15.4 us -> 29.3 us
  waiting for transfers between devices: 671 us -> 680 us
    all_gather x0 -> x2, waiting for transfers between devices: none -> 111 us  [on_device(): lax.all_gather(jnp.dot(attended, out_weight, preferred_element_type=jnp.f...]
    psum x2 -> x0, waiting for transfers between devices: 101 us -> none  [on_device(): lax.psum(jnp.dot(attended, out_weight, preferred_element_type=jnp.float32...]
    reduce_sum x0 -> x2, other arithmetic: none -> 13.8 us  [on_device(): jnp.sum(lax.all_gather(jnp.dot(attended, out_weight, preferred_element_ty...]
where the time goes in v1:
time: 812 us; the launch traced here: 811 us
  waiting for transfers between devices  680 us (84%)
  matrix products  43.5 us (5%)
  local copies, waits for them, and re-layouts  31.3 us (4%)
  other arithmetic  29.3 us (4%)
  between operations  13.8 us (2%)
  starting transfers between devices  13.7 us (2%)
    all_gather x1, waiting for transfers between devices, on_device(): lax.all_gather(w_key, 'sp', axis=1, tiled=True)  146 us
    all_gather x1, waiting for transfers between devices, on_device(): lax.all_gather(w_query, 'sp', axis=1, tiled=True)  146 us
    all_gather x1, waiting for transfers between devices, on_device(): lax.all_gather(w_value, 'sp', axis=1, tiled=True)  140 us
    all_gather x1, waiting for transfers between devices, on_device(): lax.all_gather(w_out, 'sp', axis=2, tiled=True)  134 us
    all_gather x2, waiting for transfers between devices, on_device(): lax.all_gather(jnp.dot(attended, out_weight, preferred_element_type=jnp.f...  111 us
  transfers between devices with their start and end apart: 10, of which 6 were waited for; matrix products, arithmetic and copies ran while one was open for 7% of the time, Pallas kernels for 0%

profile of v1, /device:TPU:0, one launch (start us, length us, event | category | flops | bytes accessed | tf_op | source)
XLA Modules:
  0.0 811.1 jit_solution(1984601489497481170)
XLA Ops:
  6.5 0.7 all-gather.11.cloned.1.call-update
  7.3 0.7 all-gather.9.cloned.1.call-update
  8.1 0.7 all-gather.13.cloned.1.call-update
  8.8 0.5 all-gather.15.cloned.1.call-update
  9.6 1.0 fusion.73
  10.7 3.8 fusion.30
  14.5 6.0 copy.16
  21.1 140.2 %all-gather.11.cloned.1.call-done = bf16[2,4096,512]{2,1,0:T(8,128)(2,1)} async-done(((bf16[2,1024,512]{2,1,0:T(8,128)(2,1)}), bf16[2,4096,512]{2,1,0:T(8,128)(2,1)}) %all-gather.11.cloned.1.call-update) | async-done | bytes 8388624 | tf_op jit(solution)/shard_map/all_gather | solution.py:65
  161.3 3.5 fusion.55
  164.7 145.9 %all-gather.9.cloned.1.call-done = bf16[2,4096,512]{2,1,0:T(8,128)(2,1)} async-done(((bf16[2,1024,512]{2,1,0:T(8,128)(2,1)}), bf16[2,4096,512]{2,1,0:T(8,128)(2,1)}) %all-gather.9.cloned.1.call-update) | async-done | bytes 8388624 | tf_op jit(solution)/shard_map/all_gather | solution.py:64
  310.7 3.5 fusion.54
  314.2 1.3 collective-permute-start.1
  315.5 5.4 collective-permute-start
  320.9 145.7 %all-gather.13.cloned.1.call-done = bf16[2,4096,512]{2,1,0:T(8,128)(2,1)} async-done(((bf16[2,1024,512]{2,1,0:T(8,128)(2,1)}), bf16[2,4096,512]{2,1,0:T(8,128)(2,1)}) %all-gather.13.cloned.1.call-update) | async-done | bytes 8388624 | tf_op jit(solution)/shard_map/all_gather | solution.py:63
  466.6 3.5 fusion.56
  470.1 2.5 pad_maximum_fusion
  472.7 4.2 gather_fusion
  476.9 3.7 slice_bitcast_fusion.19
  480.5 0.7 copy-done.2
  481.2 1.0 fusion.93
  482.2 0.7 fusion.16
  483.0 1.0 fusion.60
  484.2 134.3 %all-gather.15.cloned.1.call-done = bf16[2,512,4096]{2,1,0:T(8,128)(2,1)} async-done(((bf16[2,512,1024]{2,1,0:T(8,128)(2,1)}), bf16[2,512,4096]{2,1,0:T(8,128)(2,1)}) %all-gather.15.cloned.1.call-update) | async-done | bytes 8388624 | tf_op jit(solution)/shard_map/all_gather | solution.py:66
  618.4 4.8 convolution_convert_fusion.1
  623.5 2.4 fusion.71
  625.9 53.9 %all-gather.17.cloned.1.call-done = bf16[1024,4096]{1,0:T(8,128)(2,1)} async-done(((bf16[256,4096]{1,0:T(8,128)(2,1)}), bf16[1024,4096]{1,0:T(8,128)(2,1)}) %all-gather.17.cloned.1.call-update) | async-done | bytes 8388624 | tf_op jit(solution)/shard_map/all_gather | solution.py:105
  679.8 6.9 reduce_sum.62
  686.7 2.5 fusion.4
  689.3 1.0 fusion.6
  690.2 4.5 fusion.58
  694.8 1.2 fusion.57
  696.1 1.3 collective-permute-start.3
  697.4 5.4 collective-permute-start.2
  702.8 3.9 fusion.28
  706.7 5.8 copy.22
  712.4 4.8 fusion.59
  717.2 1.0 reshape.189
  718.2 2.4 pad_maximum_fusion.1
  720.6 4.2 gather_fusion.1
  724.8 3.1 slice_bitcast_fusion.17
  728.3 1.0 fusion.94
  729.3 0.7 fusion.17
  730.0 1.0 fusion.65
  731.5 1.5 slice-done.1
  733.0 2.7 convolution_convert_fusion
  735.7 57.0 %all-gather.19.cloned.1.call-done = bf16[1024,4096]{1,0:T(8,128)(2,1)} async-done(((bf16[256,4096]{1,0:T(8,128)(2,1)}), bf16[1024,4096]{1,0:T(8,128)(2,1)}) %all-gather.19.cloned.1.call-update) | async-done | bytes 8388624 | tf_op jit(solution)/shard_map/all_gather | solution.py:105
  792.6 7.0 reduce_sum.65
  799.6 4.7 fusion.7
  (53 shorter events, 2.5 us)
Async XLA Ops:
  6.5 2.9 copy-start.7
  6.5 154.7 %all-gather.11.cloned.1.call-start = ((), (), s32[]{:S(2)}) async-start(), calls=%async_computation.1 | async-start | bytes 10485760 | tf_op jit(solution)/shard_map/all_gather | solution.py:65
  7.3 303.4 %all-gather.9.cloned.1.call-start = ((), (), s32[]{:S(2)}) async-start(), calls=%async_computation | async-start | bytes 10485760 | tf_op jit(solution)/shard_map/all_gather | solution.py:64
  8.0 458.5 %all-gather.13.cloned.1.call-start = ((), (), s32[]{:S(2)}) async-start(), calls=%async_computation.2 | async-start | bytes 10485760 | tf_op jit(solution)/shard_map/all_gather | solution.py:63
  8.7 609.7 %all-gather.15.cloned.1.call-start = ((), (), s32[]{:S(2)}) async-start(), calls=%async_computation.3 | async-start | bytes 10485760 | tf_op jit(solution)/shard_map/all_gather | solution.py:66
  9.3 670.5 %all-gather.17.cloned.1.call-start = ((), (), s32[]{:S(2)}) async-start(), calls=%async_computation.4 | async-start | bytes 10485760 | tf_op jit(solution)/shard_map/all_gather | solution.py:105
  14.5 6.0 copy-start
  14.5 6.6 copy-start.6
  314.2 155.9 %collective-permute-start.1 = (bf16[4,64,1024]{2,1,0:T(8,128)(2,1)S(1)}, bf16[4,64,1024]{2,1,0:T(8,128)(2,1)}, u32[]{:S(2)}, u32[]{:S(2)}) collective-permute-start(bf16[4,64,1024]{2,1,0:T(8,128)(2,1)S(1)} %bitcast.154), channel_id=1, source_target_pairs={{4,0},{8,4},{12,8},{5,1},{9,5},{13,9},{6,2},{10,6},{14,10},{7,3},{... | collective-permute-start | bytes 1572872 | tf_op jit(solution)/shard_map/ppermute | solution.py:22
  315.5 154.6 %collective-permute-start = (bf16[4,64,1024]{2,1,0:T(8,128)(2,1)S(1)}, bf16[4,64,1024]{2,1,0:T(8,128)(2,1)}, u32[]{:S(2)}, u32[]{:S(2)}) collective-permute-start(bf16[4,64,1024]{2,1,0:T(8,128)(2,1)S(1)} %bitcast.155), channel_id=1, source_target_pairs={{0,4},{4,8},{8,12},{1,5},{5,9},{9,13},{2,6},{6,10},{10,14},{3,7},{... | collective-permute-start | bytes 1572872 | tf_op jit(solution)/shard_map/ppermute | solution.py:19
  476.9 4.3 copy-start.2
  623.2 169.4 %all-gather.19.cloned.1.call-start = ((), (), s32[]{:S(2)}) async-start(), calls=%async_computation.5 | async-start | bytes 10485760 | tf_op jit(solution)/shard_map/all_gather | solution.py:105
  686.7 2.5 copy-start.1
  689.2 5.5 slice-start.2
  690.2 4.5 copy-start.5
  690.2 4.6 slice-start.3
  694.8 8.0 copy-start.4
  696.1 22.1 %collective-permute-start.3 = (bf16[4,64,1024]{2,1,0:T(8,128)(2,1)S(1)}, bf16[4,64,1024]{2,1,0:T(8,128)(2,1)S(1)}, u32[]{:S(2)}, u32[]{:S(2)}) collective-permute-start(bf16[4,64,1024]{2,1,0:T(8,128)(2,1)S(1)} %bitcast.151), channel_id=1, source_target_pairs={{4,0},{8,4},{12,8},{5,1},{9,5},{13,9},{6,2},{10,6},{14,10},{7,3},{... | collective-permute-start | bytes 1572872 | tf_op jit(solution)/shard_map/ppermute | solution.py:22
  697.4 20.8 %collective-permute-start.2 = (bf16[4,64,1024]{2,1,0:T(8,128)(2,1)S(1)}, bf16[4,64,1024]{2,1,0:T(8,128)(2,1)}, u32[]{:S(2)}, u32[]{:S(2)}) collective-permute-start(bf16[4,64,1024]{2,1,0:T(8,128)(2,1)S(1)} %bitcast.152), channel_id=1, source_target_pairs={{0,4},{4,8},{8,12},{1,5},{5,9},{9,13},{2,6},{6,10},{10,14},{3,7},{... | collective-permute-start | bytes 1572872 | tf_op jit(solution)/shard_map/ppermute | solution.py:19
  724.8 3.4 copy-start.3
  729.3 2.2 slice-start
  730.0 2.9 slice-start.1
Sparse Core Ops, SparseCore 0:
  8.9 152.3 all-gather.10
  162.8 147.7 all-gather.8
  312.2 154.2 all-gather.12
  468.0 150.4 all-gather.14
  623.4 56.4 all-gather.16
  735.8 56.8 all-gather.18
